TPU v7x, 32 devices: a whole 2x2x4 slice. The times are simulated.
32 devices in a mesh: sp: 8 (over z, x), tp: 4 (over y, core).
Axes of the slice: x: 2, y: 2, z: 4, core: 2. Of those that a mesh axis runs over, the one named last changes fastest.
Arguments:
- residual: bfloat16 [6144, 2048], P('sp'), may hold values from -6 to 6
- queries: bfloat16 [6144, 1024], P('sp', 'tp'), may hold values from -12 to 12
- keys: bfloat16 [6144, 512], P('sp', 'tp'), may hold values from -6 to 6
- values: bfloat16 [6144, 512], P('sp', 'tp'), may hold values from -36 to 36
- segments: int32 [6144], P('sp'), may hold values from 0 to 3, never falling along the last dimension, each value on 1 to 3072 neighbouring positions
- sink: float32 [16], P('tp'), may hold values from 3 to 7
- out_weight: bfloat16 [1024, 2048], replicated, may hold values from -0.1875 to 0.1875
- norm_gain_one: float32 [2048], replicated, may hold values from 0.1 to 1.9
- group: int32 [6144], P('sp'), may hold values from 0 to 3, as said below
- member: int32 [6144, 2], P('sp'), may hold values from 0 to 7, as said below
- route_weight: float32 [6144, 2], P('sp'), may hold values from 0.25 to 1
- gate_weight: bfloat16 [32, 2048, 1024], P('sp', None, 'tp'), may hold values from -0.125 to 0.125
- up_weight: bfloat16 [32, 2048, 1024], P('sp', None, 'tp'), may hold values from -0.125 to 0.125
- down_weight: bfloat16 [32, 1024, 2048], P('sp', None, 'tp'), may hold values from -0.1875 to 0.1875
- norm_gain_two: float32 [2048], P('tp'), may hold values from 0.1 to 1.9
Outputs:
- output: bfloat16 [6144, 2048], P('sp', 'tp')
Inputs may be any that keep to these rules, and one draw needn't show every extreme that they name: In every aligned block of 192 rows no expert (group * 8 + member) is named by more than 24 rows, and one expert, the same in all blocks of a draw, is named by exactly 24 rows of every block. `member`: the 2 members of a row differ.
All inputs are finite; a program needn't handle non-finite values.
Results may differ from a plain program's by a relative error of at most 0.0059.
Values may be sent and summed in bfloat16 or wider, within the bound.
A program may use at most 128 MiB of HBM per device.

v0:
```python
import math
import jax
import jax.numpy as jnp
from jax import lax
from jax.sharding import PartitionSpec as P

HEAD_DIM = 64
HALF = 128
PER_GROUP = 8
ALPHA = 2.0**0.25
EPS = 1e-05


def with_halo(block, sides, width):
    for axis, dim in sides:
        count = lax.axis_size(axis)
        forward = [(i, i + 1) for i in range(count - 1)]
        backward = [(target, source) for source, target in forward]
        low = lax.ppermute(
            lax.slice_in_dim(block, block.shape[dim] - width, None, axis=dim), axis, forward
        )
        high = lax.ppermute(lax.slice_in_dim(block, 0, width, axis=dim), axis, backward)
        block = jnp.concatenate([low, block, high], axis=dim)
    return block


def layer_norm(summed, norm_gain):
    mean_value = jnp.mean(summed, -1, keepdims=True)
    variance = jnp.mean(jnp.square(summed - mean_value), -1, keepdims=True)
    return ((summed - mean_value) * lax.rsqrt(variance + EPS) * norm_gain).astype(jnp.bfloat16)


def shards(
    residual,
    queries,
    keys,
    values,
    segments,
    sink,
    out_weight,
    norm_gain_one,
    group,
    member,
    route_weight,
    gate_weight,
    up_weight,
    down_weight,
    norm_gain_two,
):
    row_count = queries.shape[0]
    sp_size = lax.axis_size("sp")
    tp_size = lax.axis_size("tp")
    kv_local = keys.shape[1] // HEAD_DIM
    heads_local = queries.shape[1] // HEAD_DIM
    group_size = heads_local // kv_local
    seq_total = row_count * sp_size
    seq_start = lax.axis_index("sp") * row_count
    joined = jnp.concatenate([keys, values], axis=1)
    padded, seg_padded = (
        with_halo(joined, (("sp", 0),), HALF),
        with_halo(segments, (("sp", 0),), HALF),
    )
    query_block = math.gcd(row_count, 512)
    key_span = query_block + 2 * HALF
    offsets = jnp.arange(key_span)[None, :] - HALF - jnp.arange(query_block)[:, None]
    in_band = jnp.abs(offsets) <= HALF
    sink_heads = sink.reshape(kv_local, group_size, 1, 1)
    query_heads = queries.reshape(row_count, kv_local, group_size, HEAD_DIM)
    key_cols = kv_local * HEAD_DIM
    pieces = []
    for number in range(row_count // query_block):
        row_low = number * query_block
        query_rows = query_heads[row_low : row_low + query_block]
        kv_rows = padded[row_low : row_low + key_span]
        key_part = kv_rows[:, :key_cols].reshape(key_span, kv_local, HEAD_DIM)
        value_part = kv_rows[:, key_cols:].reshape(key_span, kv_local, HEAD_DIM)
        key_place = seq_start + row_low - HALF + jnp.arange(key_span)
        inside = (key_place >= 0) & (key_place < seq_total)
        same_doc = (
            segments[row_low : row_low + query_block, None]
            == seg_padded[None, row_low : row_low + key_span]
        )
        allowed = in_band & same_doc & inside[None, :]
        scores = jnp.einsum(
            "qkgd,ckd->kgqc", query_rows, key_part, preferred_element_type=jnp.float32
        ) * HEAD_DIM ** (-0.5)
        masked = jnp.where(allowed, scores, -1e30)
        peak = jnp.maximum(jnp.max(masked, -1, keepdims=True), sink_heads)
        raised = jnp.where(allowed, jnp.exp(masked - peak), 0.0)
        denominator = jnp.sum(raised, -1, keepdims=True) + jnp.exp(sink_heads - peak)
        weights = (raised / denominator).astype(jnp.bfloat16)
        attended_part = jnp.einsum(
            "kgqc,ckd->qkgd", weights, value_part, preferred_element_type=jnp.float32
        )
        pieces.append(
            attended_part.reshape(query_block, heads_local * HEAD_DIM).astype(jnp.bfloat16)
        )
    attended = jnp.concatenate(pieces, 0)
    width = out_weight.shape[1]
    weight_rows = out_weight
    mixed = jnp.dot(
        lax.all_gather(attended, "tp", axis=1, tiled=True),
        weight_rows,
        preferred_element_type=jnp.float32,
    )
    pre_one = ALPHA * residual.astype(jnp.float32) + mixed
    normed = layer_norm(pre_one, norm_gain_one)
    experts_local = gate_weight.shape[0]
    expert_count = experts_local * sp_size
    picks_count = member.shape[1]
    block_rows = row_count // tp_size
    capacity = max(2, block_rows // 8)
    expert_ids = (group[:, None] * PER_GROUP + member).reshape(tp_size, block_rows * picks_count)
    onehot_table = (expert_ids[:, :, None] == jnp.arange(expert_count)[None, None, :]).astype(
        jnp.int32
    )
    ranks = jnp.sum((jnp.cumsum(onehot_table, 1) - 1) * onehot_table, 2)
    owner = expert_ids // experts_local
    local_ids = expert_ids % experts_local
    block_ids = jnp.arange(tp_size)[:, None]
    slot_all = ((local_ids * sp_size + owner) * tp_size + block_ids) * capacity + ranks
    copy_rows = (
        jnp.arange(row_count * picks_count).reshape(tp_size, block_rows * picks_count)
        // picks_count
    )
    extended = jnp.concatenate([normed, jnp.zeros((1, width), jnp.bfloat16)], 0)
    tp_place = lax.axis_index("tp")
    slot_own_base = (local_ids * sp_size + owner) * capacity + ranks
    own_slots = lax.dynamic_index_in_dim(slot_own_base, tp_place, 0, keepdims=False)
    own_rows = lax.dynamic_index_in_dim(copy_rows, tp_place, 0, keepdims=False)
    slot_count = experts_local * sp_size * capacity
    source = jnp.full((slot_count,), row_count, jnp.int32).at[own_slots].set(own_rows)
    outgoing = extended[source].reshape(experts_local, sp_size, capacity, width)
    received = lax.all_to_all(outgoing, "sp", split_axis=1, concat_axis=1, tiled=True)
    arrived = lax.all_gather(received, "tp", axis=2, tiled=True)
    expert_rows = arrived.reshape(experts_local, sp_size * tp_size * capacity, width)
    gate_part = jnp.einsum(
        "esd,edf->esf", expert_rows, gate_weight, preferred_element_type=jnp.float32
    )
    up_part = jnp.einsum("esd,edf->esf", expert_rows, up_weight, preferred_element_type=jnp.float32)
    hidden = (jax.nn.silu(gate_part) * up_part).astype(jnp.bfloat16)
    column_width = down_weight.shape[2]
    weight_rows = down_weight
    produced = jnp.einsum(
        "esf,efc->esc",
        lax.all_gather(hidden, "tp", axis=2, tiled=True),
        weight_rows,
        preferred_element_type=jnp.float32,
    ).astype(jnp.bfloat16)
    returned = lax.all_to_all(
        produced.reshape(experts_local, sp_size, tp_size * capacity, column_width),
        "sp",
        split_axis=1,
        concat_axis=1,
        tiled=True,
    )
    result_rows = returned.reshape(-1, column_width)
    picked = result_rows[slot_all.reshape(row_count, picks_count)]
    combined = jnp.sum(route_weight[:, :, None] * picked.astype(jnp.float32), 1)
    column_start = lax.axis_index("tp") * column_width
    normed_part = lax.dynamic_slice_in_dim(normed, column_start, column_width, 1)
    pre_two = ALPHA * normed_part.astype(jnp.float32) + combined
    sums, squares = lax.psum((jnp.sum(pre_two, -1), jnp.sum(pre_two * pre_two, -1)), "tp")
    mean_value = (sums / width)[:, None]
    variance = (squares / width)[:, None] - mean_value * mean_value
    return ((pre_two - mean_value) * lax.rsqrt(variance + EPS) * norm_gain_two).astype(jnp.bfloat16)


def solution(mesh):
    in_specs = (
        P("sp", None),
        P("sp", "tp"),
        P("sp", "tp"),
        P("sp", "tp"),
        P("sp"),
        P("tp"),
        P(),
        P(),
        P("sp"),
        P("sp", None),
        P("sp", None),
        P("sp", None, "tp"),
        P("sp", None, "tp"),
        P("sp", None, "tp"),
        P("tp"),
    )
    out_specs = P("sp", "tp")
    return jax.shard_map(shards, mesh=mesh, in_specs=in_specs, out_specs=out_specs, check_vma=False)
```

profile of v0, /device:TPU:0, one launch (start us, length us, event | category | flops | bytes accessed | tf_op | source)
XLA Modules:
  0.0 423.6 jit_solution(6903600422677034529)
XLA Ops:
  6.6 0.8 fusion.54
  7.4 4.9 %collective-permute-start.1 = (s32[128]{0:T(128)S(1)}, s32[128]{0:T(128)S(1)}, u32[]{:S(2)}, u32[]{:S(2)}) collective-permute-start(s32[128]{0:T(128)S(1)} %get-tuple-element.30), channel_id=1, source_target_pairs={{0,4},{4,8},{8,12},{12,16},{16,20},{20,24},{24,28},{1,5},{5,9},{9,... | collective-permute-start | bytes 1544 | tf_op jit(solution)/shard_map/ppermute | solution.py:19
  12.3 1.3 collective-permute-start.3
  13.6 1.0 constant_dynamic-update-slice_fusion.1
  14.5 1.0 constant_dynamic-update-slice_fusion
  15.5 0.6 fusion.52
  16.1 4.5 %collective-permute-start = (bf16[128,256]{1,0:T(8,128)(2,1)}, bf16[128,256]{1,0:T(8,128)(2,1)S(1)}, u32[]{:S(2)}, u32[]{:S(2)}) collective-permute-start(bf16[128,256]{1,0:T(8,128)(2,1)} %get-tuple-element.20), channel_id=1, source_target_pairs={{0,4},{4,8},{8,12},{12,16},{16,20},{20,24},{24,28},{1,5},{5,9},{9,... | collective-permute-start | bytes 196616 | tf_op jit(solution)/shard_map/ppermute | solution.py:19
  20.7 1.3 collective-permute-start.2
  22.0 0.7 slice.96
  22.7 0.8 fusion.55
  23.5 1.1 fusion.51
  24.8 0.8 copy.52
  26.0 0.7 and_and_fusion.2
  26.7 0.5 fusion.1
  27.2 0.6 copy-done.7
  27.9 1.5 pad_maximum_fusion.3
  29.4 1.0 copy.47
  30.4 0.8 copy.46
  31.4 0.5 fusion
  32.0 0.5 fusion.3
  32.6 0.5 fusion.2
  33.2 0.8 convolution_convert_fusion.3
  34.0 0.5 fusion.4
  34.5 0.5 fusion.5
  35.1 0.8 convolution_convert_fusion.2
  36.0 0.7 convolution_convert_fusion.1
  36.8 0.8 pad_maximum_fusion
  37.6 0.2 copy.59
  37.9 0.2 broadcast_add_fusion
  38.0 0.2 reshape.202
  38.3 0.3 eq.76
  38.5 3.5 reduce-window.6
  42.6 3.1 scatter_custom_fusion
  45.7 14.9 %all-gather.4.cloned.1.call-done = bf16[768,1024]{0,1:T(8,128)(2,1)} async-done(((bf16[768,256]{0,1:T(8,128)(2,1)}), bf16[768,1024]{0,1:T(8,128)(2,1)}) %all-gather.4.cloned.1.call-update) | async-done | bytes 1572880 | tf_op jit(solution)/shard_map/all_gather | solution.py:102
  60.6 7.8 %fusion.56 = (f32[768]{0:T(1024)S(1)}, f32[768,2048]{1,0:T(8,128)S(1)}) fusion(bf16[768,1024]{0,1:T(8,128)(2,1)} %all-gather.4.cloned.1.call-done, bf16[1024,2048]{1,0:T(8,128)(2,1)} %param.21, bf16[768,2048]{1,0:T(8,128)(2,1)} %param.15), kind=kOutput, calls=%fused_computation.146 | convolution fusion | flops 3227516160 | bytes 15207424 | tf_op jit(solution)/shard_map/dot_general | solution.py:101
  68.5 0.8 multiply_reduce_fusion
  69.3 0.9 multiply_convert_fusion
  70.1 1.7 copy-done
  71.8 0.2 concatenate.29
  72.0 4.3 %gather_fusion = bf16[768,2048]{1,0:T(8,128)(2,1)} fusion(bf16[769,2048]{1,0:T(8,128)(2,1)S(1)} %concatenate.29, s32[1024]{0:T(1024)S(1)} %pad_clamp_fusion.1), kind=kCustom, calls=%fused_computation | custom fusion | bytes 6294528 | tf_op jit(solution)/shard_map/gather | solution.py:133
  76.3 2.3 copy.63
  78.6 76.5 %all_to_all.10 = bf16[4,8,24,2048]{3,2,0,1:T(8,128)(2,1)} all-to-all(bf16[4,8,24,2048]{3,2,0,1:T(8,128)(2,1)S(1)} %copy.63), channel_id=1, replica_groups=mesh['sp'=8,'tp'=4] {'sp'}, dimensions={1} | all-to-all | bytes 6291456 | tf_op jit(solution)/shard_map/all_to_all | solution.py:134
  155.1 0.3 all-gather.8.cloned.1.call-start
  155.4 80.1 %all-gather.6.cloned.1.call-done = bf16[4,8,96,2048]{3,2,0,1:T(8,128)(2,1)} async-done(((bf16[4,8,24,2048]{3,2,0,1:T(8,128)(2,1)}), bf16[4,8,96,2048]{3,2,0,1:T(8,128)(2,1)}) %all-gather.6.cloned.1.call-update) | async-done | bytes 12582928 | tf_op jit(solution)/shard_map/all_gather | solution.py:135
  235.5 6.4 %copy.64 = bf16[4,8,96,2048]{3,2,1,0:T(8,128)(2,1)S(1)} copy(bf16[4,8,96,2048]{3,2,0,1:T(8,128)(2,1)} %all-gather.6.cloned.1.call-done) | data formatting | bytes 25165824 | tf_op jit(solution)/shard_map/all_gather | solution.py:135
  241.9 5.1 %fusion.57 = f32[4,768,256]{2,1,0:T(8,128)} fusion(bf16[4,768,2048]{2,1,0:T(8,128)(2,1)S(1)} %bitcast.120, bf16[4,2048,256]{2,1,0:T(8,128)(2,1)S(1)} %copy-done.14), kind=kOutput, calls=%fused_computation.147 | convolution fusion | flops 3221225472 | bytes 19922944 | tf_op jit(solution)/shard_map/esd,edf->esf/dot_general | solution.py:137
  247.1 7.4 %multiply_convert_fusion.1 = bf16[4,768,256]{2,1,0:T(8,128)(2,1)} fusion(f32[4,768,256]{2,1,0:T(8,128)} %fusion.57, bf16[4,768,2048]{2,1,0:T(8,128)(2,1)S(1)} %bitcast.121, bf16[4,2048,256]{2,1,0:T(8,128)(2,1)} %param.27), kind=kOutput, calls=%fused_computation.7 | convolution fusion | flops 3225944064 | bytes 21495808 | tf_op jit(solution)/shard_map/esd,edf->esf/dot_general | solution.py:140
  254.5 47.3 %all-gather.8.cloned.1.call-done = bf16[4,768,1024]{2,1,0:T(8,128)(2,1)} async-done(((bf16[4,768,256]{2,1,0:T(8,128)(2,1)}), bf16[4,768,1024]{2,1,0:T(8,128)(2,1)}) %all-gather.8.cloned.1.call-update) | async-done | bytes 6291472 | tf_op jit(solution)/shard_map/all_gather | solution.py:146
  301.8 7.4 %convolution_convert_fusion = bf16[4,768,512]{2,1,0:T(8,128)(2,1)S(1)} fusion(bf16[4,768,1024]{2,1,0:T(8,128)(2,1)} %all-gather.8.cloned.1.call-done, bf16[4,1024,512]{2,1,0:T(8,128)(2,1)} %param.28), kind=kOutput, calls=%fused_computation.8 | convolution fusion | flops 3222798336 | bytes 13631488 | tf_op jit(solution)/shard_map/esf,efc->esc/dot_general | solution.py:144
  309.3 2.0 copy.65
  311.3 5.7 %all-to-all-start.1 = ((bf16[4,8,96,512]{3,2,0,1:T(8,128)(2,1)}), bf16[4,8,96,512]{3,2,0,1:T(8,128)(2,1)}, u32[]{:S(2)}, u32[]{:S(2)}) async-start(bf16[4,8,96,512]{3,2,0,1:T(8,128)(2,1)} %copy.65), calls=%async_computation.1 | async-start | bytes 6291456 | tf_op jit(solution)/shard_map/all_to_all | solution.py:150
  316.9 0.3 reduce_sum.89
  317.4 0.5 compare_select_fusion
  317.9 0.2 reshape.221
  318.1 0.2 copy.58
  318.3 69.8 %all-to-all-done.1 = bf16[4,8,96,512]{3,2,0,1:T(8,128)(2,1)} async-done(((bf16[4,8,96,512]{3,2,0,1:T(8,128)(2,1)}), bf16[4,8,96,512]{3,2,0,1:T(8,128)(2,1)}, u32[]{:S(2)}, u32[]{:S(2)}) %all-to-all-start.1) | async-done | bytes 3145760 | tf_op jit(solution)/shard_map/all_to_all | solution.py:150
  388.1 2.2 copy.66
  390.4 5.4 %gather_fusion.1 = bf16[1536,512]{1,0:T(8,128)(2,1)} fusion(bf16[3072,512]{1,0:T(8,128)(2,1)S(1)} %bitcast.119, s32[2048]{0:T(1024)S(1)} %pad_clamp_fusion), kind=kCustom, calls=%fused_computation.1 | custom fusion | bytes 3151872 | tf_op jit(solution)/shard_map/gather | solution.py:158
  395.8 4.8 %reshape.238 = f32[768,2,512]{2,1,0:T(2,128)} reshape(bf16[1536,512]{1,0:T(8,128)(2,1)} %gather_fusion.1) | data formatting | bytes 4718592 | tf_op jit(solution)/shard_map/convert_element_type | solution.py:159
  400.6 6.1 %multiply_reduce_fusion.1 = f32[768,512]{1,0:T(8,128)S(1)} fusion(f32[768,2,512]{2,1,0:T(2,128)} %reshape.238, f32[768,2]{1,0:T(8,128)S(1)} %copy.58), kind=kLoop, calls=%fused_computation.6 | loop fusion | flops 1179648 | bytes 4724736 | tf_op jit(solution)/shard_map/reduce_sum | solution.py:159
  406.7 1.2 copy-done.2
  407.9 0.4 fusion.16
  408.3 6.1 %all-reduce.1 = (f32[768]{0:T(1024)S(1)}, f32[768]{0:T(1024)S(1)}) all-reduce(f32[768]{0:T(1024)S(1)} %get-tuple-element.6, f32[768]{0:T(1024)S(1)} %get-tuple-element.5), channel_id=1, replica_groups=mesh['sp'=8,'tp'=4] {'tp'}, use_global_device_ids=true, to_apply=%region_16.17 | all-reduce | flops 1536 | bytes 12288 | tf_op jit(solution)/shard_map/psum | solution.py:163
  414.4 2.6 multiply_convert_fusion.2
  (81 shorter events, 2.0 us)
Async XLA Ops:
  6.5 19.4 %copy-start.8 = (s32[768]{0:T(1024)S(1)}, s32[768]{0:T(1024)}, u32[]{:S(2)}) copy-start(s32[768]{0:T(1024)} %param.19) | copy-start | bytes 9220
  6.5 18.1 %slice-start = ((bf16[768,128]{1,0:T(8,128)(2,1)}), bf16[512,128]{1,0:T(8,128)(2,1)S(1)}, s32[]{:S(2)}) async-start(bf16[768,128]{1,0:T(8,128)(2,1)} %param.17), calls=%async_computation.5 | async-start | bytes 262144 | tf_op jit(solution)/shard_map/slice | solution.py:75
  6.5 18.3 %slice-start.1 = ((bf16[768,128]{1,0:T(8,128)(2,1)}), bf16[512,128]{1,0:T(8,128)(2,1)S(1)}, s32[]{:S(2)}) async-start(bf16[768,128]{1,0:T(8,128)(2,1)} %param.18), calls=%async_computation.6 | async-start | bytes 262144 | tf_op jit(solution)/shard_map/slice | solution.py:76
  6.5 18.0 %copy-start.15 = (f32[4]{0:T(128)S(1)}, f32[4]{0:T(128)}, u32[]{:S(2)}) copy-start(f32[4]{0:T(128)} %param.20) | copy-start | bytes 52
  6.5 54.1 %all-gather.4.cloned.1.call-start = ((), (), s32[]{:S(2)}) async-start(), calls=%async_computation.2 | async-start | bytes 1966080 | tf_op jit(solution)/shard_map/all_gather | solution.py:102
  7.4 18.5 %collective-permute-start.1 = (s32[128]{0:T(128)S(1)}, s32[128]{0:T(128)S(1)}, u32[]{:S(2)}, u32[]{:S(2)}) collective-permute-start(s32[128]{0:T(128)S(1)} %get-tuple-element.30), channel_id=1, source_target_pairs={{0,4},{4,8},{8,12},{12,16},{16,20},{20,24},{24,28},{1,5},{5,9},{9,... | collective-permute-start | bytes 1544 | tf_op jit(solution)/shard_map/ppermute | solution.py:19
  12.3 13.6 %collective-permute-start.3 = (s32[128]{0:T(128)S(1)}, s32[128]{0:T(128)S(1)}, u32[]{:S(2)}, u32[]{:S(2)}) collective-permute-start(s32[128]{0:T(128)S(1)} %get-tuple-element.31), channel_id=1, source_target_pairs={{4,0},{8,4},{12,8},{16,12},{20,16},{24,20},{28,24},{5,1},{9,5},{13... | collective-permute-start | bytes 1544 | tf_op jit(solution)/shard_map/ppermute | solution.py:22
  16.1 11.1 %collective-permute-start = (bf16[128,256]{1,0:T(8,128)(2,1)}, bf16[128,256]{1,0:T(8,128)(2,1)S(1)}, u32[]{:S(2)}, u32[]{:S(2)}) collective-permute-start(bf16[128,256]{1,0:T(8,128)(2,1)} %get-tuple-element.20), channel_id=1, source_target_pairs={{0,4},{4,8},{8,12},{12,16},{16,20},{20,24},{24,28},{1,5},{5,9},{9,... | collective-permute-start | bytes 196616 | tf_op jit(solution)/shard_map/ppermute | solution.py:19
  20.7 7.2 %collective-permute-start.2 = (bf16[128,256]{1,0:T(8,128)(2,1)S(1)}, bf16[128,256]{1,0:T(8,128)(2,1)}, u32[]{:S(2)}, u32[]{:S(2)}) collective-permute-start(bf16[128,256]{1,0:T(8,128)(2,1)S(1)} %get-tuple-element.21), channel_id=1, source_target_pairs={{4,0},{8,4},{12,8},{16,12},{20,16},{24,20},{28,24},{5,1},{9,5},{13... | collective-permute-start | bytes 196616 | tf_op jit(solution)/shard_map/ppermute | solution.py:22
  27.2 0.6 copy-start.7
  32.0 1.2 copy-start.6
  35.1 0.9 copy-start.5
  36.0 1.6 copy-start.10
  36.0 1.8 copy-start.12
  37.6 197.9 %all-gather.6.cloned.1.call-start = ((), (), s32[]{:S(2)}) async-start(), calls=%async_computation.3 | async-start | bytes 15728640 | tf_op jit(solution)/shard_map/all_gather | solution.py:135
  37.8 30.6 %copy-start.3 = (s32[768,2]{1,0:T(8,128)}, s32[768,2]{1,0:T(8,128)S(1)}, u32[]{:S(2)}) copy-start(s32[768,2]{1,0:T(8,128)S(1)} %copy.59) | copy-start | bytes 18436
  68.5 0.8 copy-start.9
  70.1 1.7 copy-start
  155.1 146.7 %all-gather.8.cloned.1.call-start = ((), (), s32[]{:S(2)}) async-start(), calls=%async_computation.4 | async-start | bytes 7864320 | tf_op jit(solution)/shard_map/all_gather | solution.py:146
  235.5 6.5 %copy-start.14 = (bf16[4,2048,256]{2,1,0:T(8,128)(2,1)S(1)}, bf16[4,2048,256]{2,1,0:T(8,128)(2,1)}, u32[]{:S(2)}) copy-start(bf16[4,2048,256]{2,1,0:T(8,128)(2,1)} %param.26) | copy-start | bytes 12582916
  311.3 6.1 %copy-start.4 = (s32[768,2]{1,0:T(8,128)S(1)}, s32[768,2]{1,0:T(8,128)}, u32[]{:S(2)}) copy-start(s32[768,2]{1,0:T(8,128)} %copy-done.3) | copy-start | bytes 18436
  311.3 6.9 %copy-start.11 = (f32[768,2]{0,1:T(2,128)S(1)}, f32[768,2]{0,1:T(2,128)}, u32[]{:S(2)}) copy-start(f32[768,2]{0,1:T(2,128)} %param.25) | copy-start | bytes 18436
  311.3 76.9 %all-to-all-start.1 = ((bf16[4,8,96,512]{3,2,0,1:T(8,128)(2,1)}), bf16[4,8,96,512]{3,2,0,1:T(8,128)(2,1)}, u32[]{:S(2)}, u32[]{:S(2)}) async-start(bf16[4,8,96,512]{3,2,0,1:T(8,128)(2,1)} %copy.65), calls=%async_computation.1 | async-start | bytes 6291456 | tf_op jit(solution)/shard_map/all_to_all | solution.py:150
  400.6 7.3 %copy-start.1 = (bf16[768,2048]{1,0:T(8,128)(2,1)S(1)}, bf16[768,2048]{1,0:T(8,128)(2,1)}, u32[]{:S(2)}) copy-start(bf16[768,2048]{1,0:T(8,128)(2,1)} %copy-done) | copy-start | bytes 9437188
  406.7 1.2 copy-start.2
  407.9 6.5 %copy-start.13 = (f32[512]{0:T(512)S(1)}, f32[512]{0:T(512)}, u32[]{:S(2)}) copy-start(f32[512]{0:T(512)} %param.29) | copy-start | bytes 6148
Sparse Core Ops, SparseCore 0:
  37.7 22.9 all-gather.3
  155.2 80.1 all-gather.5
  254.6 47.1 all-gather.7
where the time goes:
time: 424 us
  waiting for transfers between devices  212 us (50%)
  blocking collectives  82.6 us (19%)
  local copies, waits for them, and re-layouts  45.3 us (11%)
  matrix products  31.6 us (7%)
  other arithmetic  20.2 us (5%)
  starting transfers between devices  18 us (4%)
  between operations  13.7 us (3%)
    all_gather x1, waiting for transfers between devices, shards(): arrived = lax.all_gather(received, 'tp', axis=2, tiled=True)  80.1 us
    all_to_all x1, blocking collectives, shards(): lax.all_to_all(outgoing, 'sp', split_axis=1, concat_axis=1, tiled=True)  76.5 us
    all_to_all x1, waiting for transfers between devices, shards(): lax.all_to_all(produced.reshape(experts_local, sp_size, tp_size * capacit...  69.8 us
    all_gather x1, waiting for transfers between devices, shards(): lax.all_gather(hidden, 'tp', axis=2, tiled=True)  47.3 us
    all_gather x1, waiting for transfers between devices, shards(): lax.all_gather(attended, 'tp', axis=1, tiled=True)  14.9 us
    ppermute x2, starting transfers between devices, with_halo(): lax.ppermute(lax.slice_in_dim(block, block.shape[dim] - width, None, axis...  9.4 us
  transfers between devices with their start and end apart: 8, of which 4 were waited for; matrix products, arithmetic and copies ran while one was open for 4% of the time, Pallas kernels for 0%

commit v1 on v0

--- a/solution.py
+++ b/solution.py
@@ -132,7 +132,9 @@
     source = jnp.full((slot_count,), row_count, jnp.int32).at[own_slots].set(own_rows)
     outgoing = extended[source].reshape(experts_local, sp_size, capacity, width)
     received = lax.all_to_all(outgoing, "sp", split_axis=1, concat_axis=1, tiled=True)
-    arrived = lax.all_gather(received, "tp", axis=2, tiled=True)
+    arrived = jnp.concatenate(
+        lax.all_to_all(jnp.stack([received] * lax.axis_size("tp")), "tp", 0, 0), axis=2
+    )
     expert_rows = arrived.reshape(experts_local, sp_size * tp_size * capacity, width)
     gate_part = jnp.einsum(
         "esd,edf->esf", expert_rows, gate_weight, preferred_element_type=jnp.float32

time: 424 us -> 487 us (1.15)
  blocking collectives: 82.6 us -> 225 us
  waiting for transfers between devices: 212 us -> 130 us
    all_to_all x0 -> x1, blocking collectives: none -> 142 us  [shards(): lax.all_to_all(jnp.stack([received] * lax.axis_size('tp')), 'tp', 0, 0)]
    all_gather x1 -> x0, waiting for transfers between devices: 80.1 us -> none  [shards(): arrived = lax.all_gather(received, 'tp', axis=2, tiled=True)]
    all_gather x1 -> x0, local copies, waits for them, and re-layouts: 6.44 us -> none  [shards(): arrived = lax.all_gather(received, 'tp', axis=2, tiled=True)]
    another operation x2 -> x3, local copies, waits for them, and re-layouts: 0.01 us -> 6.18 us  [the longest x1 6.17 us: shards(): jnp.stack([received] * lax.axis_size('tp'))]
  transfers between devices with their start and end apart: 8 -> 7, of which waited for: 4 -> 3; matrix products, arithmetic and copies ran while one was open for 4% -> 4% of each run, Pallas kernels for 0% -> 0%
where the time goes in v1:
time: 487 us; the launch traced here: 486 us
  blocking collectives  225 us (46%)
  waiting for transfers between devices  130 us (27%)
  local copies, waits for them, and re-layouts  47.4 us (10%)
  matrix products  31.6 us (6%)
  other arithmetic  20.2 us (4%)
  starting transfers between devices  17.7 us (4%)
  between operations  14 us (3%)
    all_to_all x1, blocking collectives, shards(): lax.all_to_all(jnp.stack([received] * lax.axis_size('tp')), 'tp', 0, 0)  142 us
    all_to_all x1, blocking collectives, shards(): lax.all_to_all(outgoing, 'sp', split_axis=1, concat_axis=1, tiled=True)  76.4 us
    all_to_all x1, waiting for transfers between devices, shards(): lax.all_to_all(produced.reshape(experts_local, sp_size, tp_size * capacit...  69.8 us
    all_gather x1, waiting for transfers between devices, shards(): lax.all_gather(hidden, 'tp', axis=2, tiled=True)  45.5 us
    all_gather x1, waiting for transfers between devices, shards(): lax.all_gather(attended, 'tp', axis=1, tiled=True)  14.9 us
  transfers between devices with their start and end apart: 7, of which 3 were waited for; matrix products, arithmetic and copies ran while one was open for 4% of the time, Pallas kernels for 0%

profile of v1, /device:TPU:0, one launch (start us, length us, event | category | flops | bytes accessed | tf_op | source)
XLA Modules:
  0.0 486.1 jit_solution(6045757087814694851)
XLA Ops:
  6.6 0.8 fusion.54
  7.4 4.9 collective-permute-start.1
  12.3 1.3 collective-permute-start.3
  13.6 1.0 constant_dynamic-update-slice_fusion.1
  14.5 1.0 constant_dynamic-update-slice_fusion
  15.5 0.6 fusion.52
  16.1 4.5 collective-permute-start
  20.7 1.3 collective-permute-start.2
  22.0 0.7 slice.96
  22.7 0.8 fusion.55
  23.5 1.1 fusion.51
  24.8 0.8 copy.52
  25.9 0.7 and_and_fusion.2
  26.7 0.5 fusion.1
  27.2 0.6 copy-done.7
  27.8 1.5 pad_maximum_fusion.3
  29.4 1.0 copy.47
  30.4 0.8 copy.46
  31.4 0.5 fusion
  32.0 0.5 fusion.3
  32.6 0.5 fusion.2
  33.2 0.8 convolution_convert_fusion.3
  34.0 0.5 fusion.4
  34.5 0.5 fusion.5
  35.1 0.8 convolution_convert_fusion.2
  36.0 0.7 convolution_convert_fusion.1
  36.8 0.8 pad_maximum_fusion
  37.6 0.2 copy.59
  38.0 0.2 reshape.204
  38.3 0.3 eq.76
  38.5 3.5 reduce-window.6
  42.6 3.1 scatter_custom_fusion
  45.7 14.9 %all-gather.3.cloned.1.call-done = bf16[768,1024]{0,1:T(8,128)(2,1)} async-done(((bf16[768,256]{0,1:T(8,128)(2,1)}), bf16[768,1024]{0,1:T(8,128)(2,1)}) %all-gather.3.cloned.1.call-update) | async-done | bytes 1572880 | tf_op jit(solution)/shard_map/all_gather | solution.py:102
  60.6 7.8 %fusion.56 = (f32[768]{0:T(1024)S(1)}, f32[768,2048]{1,0:T(8,128)S(1)}) fusion(bf16[768,1024]{0,1:T(8,128)(2,1)} %all-gather.3.cloned.1.call-done, bf16[1024,2048]{1,0:T(8,128)(2,1)} %param.21, bf16[768,2048]{1,0:T(8,128)(2,1)} %param.15), kind=kOutput, calls=%fused_computation.146 | convolution fusion | flops 3227516160 | bytes 15207424 | tf_op jit(solution)/shard_map/dot_general | solution.py:101
  68.5 0.8 multiply_reduce_fusion
  69.2 0.9 multiply_convert_fusion
  70.1 1.7 copy-done
  71.8 0.2 concatenate.29
  72.0 4.3 gather_fusion
  76.3 2.3 copy.63
  78.6 76.4 %all_to_all.15 = bf16[4,8,24,2048]{3,2,0,1:T(8,128)(2,1)S(1)} all-to-all(bf16[4,8,24,2048]{3,2,0,1:T(8,128)(2,1)S(1)} %copy.63), channel_id=1, replica_groups=mesh['sp'=8,'tp'=4] {'sp'}, dimensions={1} | all-to-all | bytes 6291456 | tf_op jit(solution)/shard_map/all_to_all | solution.py:134
  155.0 0.2 copy.64
  155.2 6.2 %stack.2 = bf16[4,4,8,24,2048]{4,3,2,1,0:T(8,128)(2,1)} broadcast(bf16[4,8,24,2048]{3,2,1,0:T(8,128)(2,1)S(1)} %copy.64), dimensions={1,2,3,4} | broadcast | bytes 15728640 | tf_op jit(solution)/shard_map/stack | solution.py:136
  161.4 142.4 %all_to_all.16 = bf16[4,4,8,24,2048]{4,3,2,1,0:T(8,128)(2,1)S(1)} all-to-all(bf16[4,4,8,24,2048]{4,3,2,1,0:T(8,128)(2,1)} %stack.2), channel_id=1, replica_groups=mesh['sp'=8,'tp'=4] {'tp'}, dimensions={0} | all-to-all | bytes 25165824 | tf_op jit(solution)/shard_map/all_to_all | solution.py:136
  303.8 1.9 copy.65
  305.7 0.3 copy-done.14
  306.0 5.2 %fusion.57 = f32[4,768,256]{2,1,0:T(8,128)} fusion(bf16[4,768,2048]{2,1,0:T(8,128)(2,1)S(1)} %bitcast.122, bf16[4,2048,256]{2,1,0:T(8,128)(2,1)S(1)} %copy-done.14), kind=kOutput, calls=%fused_computation.147 | convolution fusion | flops 3221225472 | bytes 19922944 | tf_op jit(solution)/shard_map/esd,edf->esf/dot_general | solution.py:139
  311.2 7.4 %multiply_convert_fusion.1 = bf16[4,768,256]{2,1,0:T(8,128)(2,1)} fusion(f32[4,768,256]{2,1,0:T(8,128)} %fusion.57, bf16[4,768,2048]{2,1,0:T(8,128)(2,1)S(1)} %bitcast.123, bf16[4,2048,256]{2,1,0:T(8,128)(2,1)} %param.27), kind=kOutput, calls=%fused_computation.7 | convolution fusion | flops 3225944064 | bytes 21495808 | tf_op jit(solution)/shard_map/esd,edf->esf/dot_general | solution.py:142
  318.6 45.5 %all-gather.5.cloned.1.call-done = bf16[4,768,1024]{2,1,0:T(8,128)(2,1)} async-done(((bf16[4,768,256]{2,1,0:T(8,128)(2,1)}), bf16[4,768,1024]{2,1,0:T(8,128)(2,1)}) %all-gather.5.cloned.1.call-update) | async-done | bytes 6291472 | tf_op jit(solution)/shard_map/all_gather | solution.py:148
  364.1 7.4 %convolution_convert_fusion = bf16[4,768,512]{2,1,0:T(8,128)(2,1)S(1)} fusion(bf16[4,768,1024]{2,1,0:T(8,128)(2,1)} %all-gather.5.cloned.1.call-done, bf16[4,1024,512]{2,1,0:T(8,128)(2,1)} %param.28), kind=kOutput, calls=%fused_computation.8 | convolution fusion | flops 3222798336 | bytes 13631488 | tf_op jit(solution)/shard_map/esf,efc->esc/dot_general | solution.py:146
  371.5 2.0 copy.66
  373.5 5.6 %all-to-all-start.2 = ((bf16[4,8,96,512]{3,2,0,1:T(8,128)(2,1)}), bf16[4,8,96,512]{3,2,0,1:T(8,128)(2,1)}, u32[]{:S(2)}, u32[]{:S(2)}) async-start(bf16[4,8,96,512]{3,2,0,1:T(8,128)(2,1)} %copy.66), calls=%async_computation.2 | async-start | bytes 6291456 | tf_op jit(solution)/shard_map/all_to_all | solution.py:152
  379.2 0.3 reduce_sum.89
  379.6 0.5 compare_select_fusion
  380.1 0.2 reshape.223
  380.6 69.8 %all-to-all-done.2 = bf16[4,8,96,512]{3,2,0,1:T(8,128)(2,1)} async-done(((bf16[4,8,96,512]{3,2,0,1:T(8,128)(2,1)}), bf16[4,8,96,512]{3,2,0,1:T(8,128)(2,1)}, u32[]{:S(2)}, u32[]{:S(2)}) %all-to-all-start.2) | async-done | bytes 3145760 | tf_op jit(solution)/shard_map/all_to_all | solution.py:152
  450.4 2.2 copy.67
  452.6 5.4 %gather_fusion.1 = bf16[1536,512]{1,0:T(8,128)(2,1)} fusion(bf16[3072,512]{1,0:T(8,128)(2,1)S(1)} %bitcast.120, s32[2048]{0:T(1024)S(1)} %pad_clamp_fusion), kind=kCustom, calls=%fused_computation.1 | custom fusion | bytes 3151872 | tf_op jit(solution)/shard_map/gather | solution.py:160
  458.0 4.7 reshape.240
  462.8 6.1 %multiply_reduce_fusion.1 = f32[768,512]{1,0:T(8,128)S(1)} fusion(f32[768,2,512]{2,1,0:T(2,128)} %reshape.240, f32[768,2]{1,0:T(8,128)S(1)} %copy.58), kind=kLoop, calls=%fused_computation.6 | loop fusion | flops 1179648 | bytes 4724736 | tf_op jit(solution)/shard_map/reduce_sum | solution.py:161
  468.9 1.1 copy-done.2
  470.1 0.4 fusion.16
  470.5 6.1 %all-reduce.1 = (f32[768]{0:T(1024)S(1)}, f32[768]{0:T(1024)S(1)}) all-reduce(f32[768]{0:T(1024)S(1)} %get-tuple-element.6, f32[768]{0:T(1024)S(1)} %get-tuple-element.5), channel_id=1, replica_groups=mesh['sp'=8,'tp'=4] {'tp'}, use_global_device_ids=true, to_apply=%region_16.17 | all-reduce | flops 1536 | bytes 12288 | tf_op jit(solution)/shard_map/psum | solution.py:165
  476.6 2.6 multiply_convert_fusion.2
  (81 shorter events, 2.3 us)
Async XLA Ops:
  6.5 19.4 %copy-start.8 = (s32[768]{0:T(1024)S(1)}, s32[768]{0:T(1024)}, u32[]{:S(2)}) copy-start(s32[768]{0:T(1024)} %param.19) | copy-start | bytes 9220
  6.5 18.1 %slice-start = ((bf16[768,128]{1,0:T(8,128)(2,1)}), bf16[512,128]{1,0:T(8,128)(2,1)S(1)}, s32[]{:S(2)}) async-start(bf16[768,128]{1,0:T(8,128)(2,1)} %param.17), calls=%async_computation.5 | async-start | bytes 262144 | tf_op jit(solution)/shard_map/slice | solution.py:75
  6.5 18.3 %slice-start.1 = ((bf16[768,128]{1,0:T(8,128)(2,1)}), bf16[512,128]{1,0:T(8,128)(2,1)S(1)}, s32[]{:S(2)}) async-start(bf16[768,128]{1,0:T(8,128)(2,1)} %param.18), calls=%async_computation.6 | async-start | bytes 262144 | tf_op jit(solution)/shard_map/slice | solution.py:76
  6.5 18.0 %copy-start.15 = (f32[4]{0:T(128)S(1)}, f32[4]{0:T(128)}, u32[]{:S(2)}) copy-start(f32[4]{0:T(128)} %param.20) | copy-start | bytes 52
  6.5 54.1 %all-gather.3.cloned.1.call-start = ((), (), s32[]{:S(2)}) async-start(), calls=%async_computation.3 | async-start | bytes 1966080 | tf_op jit(solution)/shard_map/all_gather | solution.py:102
  7.4 18.5 %collective-permute-start.1 = (s32[128]{0:T(128)S(1)}, s32[128]{0:T(128)S(1)}, u32[]{:S(2)}, u32[]{:S(2)}) collective-permute-start(s32[128]{0:T(128)S(1)} %get-tuple-element.30), channel_id=1, source_target_pairs={{0,4},{4,8},{8,12},{12,16},{16,20},{20,24},{24,28},{1,5},{5,9},{9,... | collective-permute-start | bytes 1544 | tf_op jit(solution)/shard_map/ppermute | solution.py:19
  12.3 13.6 %collective-permute-start.3 = (s32[128]{0:T(128)S(1)}, s32[128]{0:T(128)S(1)}, u32[]{:S(2)}, u32[]{:S(2)}) collective-permute-start(s32[128]{0:T(128)S(1)} %get-tuple-element.31), channel_id=1, source_target_pairs={{4,0},{8,4},{12,8},{16,12},{20,16},{24,20},{28,24},{5,1},{9,5},{13... | collective-permute-start | bytes 1544 | tf_op jit(solution)/shard_map/ppermute | solution.py:22
  16.1 11.1 %collective-permute-start = (bf16[128,256]{1,0:T(8,128)(2,1)}, bf16[128,256]{1,0:T(8,128)(2,1)S(1)}, u32[]{:S(2)}, u32[]{:S(2)}) collective-permute-start(bf16[128,256]{1,0:T(8,128)(2,1)} %get-tuple-element.20), channel_id=1, source_target_pairs={{0,4},{4,8},{8,12},{12,16},{16,20},{20,24},{24,28},{1,5},{5,9},{9,... | collective-permute-start | bytes 196616 | tf_op jit(solution)/shard_map/ppermute | solution.py:19
  20.7 7.2 %collective-permute-start.2 = (bf16[128,256]{1,0:T(8,128)(2,1)S(1)}, bf16[128,256]{1,0:T(8,128)(2,1)}, u32[]{:S(2)}, u32[]{:S(2)}) collective-permute-start(bf16[128,256]{1,0:T(8,128)(2,1)S(1)} %get-tuple-element.21), channel_id=1, source_target_pairs={{4,0},{8,4},{12,8},{16,12},{20,16},{24,20},{28,24},{5,1},{9,5},{13... | collective-permute-start | bytes 196616 | tf_op jit(solution)/shard_map/ppermute | solution.py:22
  27.2 0.6 copy-start.7
  32.0 1.2 copy-start.6
  35.1 0.9 copy-start.5
  36.0 1.6 copy-start.10
  36.0 1.8 copy-start.12
  37.6 326.5 %all-gather.5.cloned.1.call-start = ((), (), s32[]{:S(2)}) async-start(), calls=%async_computation.4 | async-start | bytes 7864320 | tf_op jit(solution)/shard_map/all_gather | solution.py:148
  37.8 30.6 %copy-start.3 = (s32[768,2]{1,0:T(8,128)}, s32[768,2]{1,0:T(8,128)S(1)}, u32[]{:S(2)}) copy-start(s32[768,2]{1,0:T(8,128)S(1)} %copy.59) | copy-start | bytes 18436
  68.5 0.8 copy-start.9
  70.1 1.7 copy-start
  303.8 2.2 copy-start.14
  373.5 6.1 %copy-start.4 = (s32[768,2]{1,0:T(8,128)S(1)}, s32[768,2]{1,0:T(8,128)}, u32[]{:S(2)}) copy-start(s32[768,2]{1,0:T(8,128)} %copy-done.3) | copy-start | bytes 18436
  373.5 6.9 %copy-start.11 = (f32[768,2]{0,1:T(2,128)S(1)}, f32[768,2]{0,1:T(2,128)}, u32[]{:S(2)}) copy-start(f32[768,2]{0,1:T(2,128)} %param.25) | copy-start | bytes 18436
  373.5 76.9 %all-to-all-start.2 = ((bf16[4,8,96,512]{3,2,0,1:T(8,128)(2,1)}), bf16[4,8,96,512]{3,2,0,1:T(8,128)(2,1)}, u32[]{:S(2)}, u32[]{:S(2)}) async-start(bf16[4,8,96,512]{3,2,0,1:T(8,128)(2,1)} %copy.66), calls=%async_computation.2 | async-start | bytes 6291456 | tf_op jit(solution)/shard_map/all_to_all | solution.py:152
  462.8 7.3 %copy-start.1 = (bf16[768,2048]{1,0:T(8,128)(2,1)S(1)}, bf16[768,2048]{1,0:T(8,128)(2,1)}, u32[]{:S(2)}) copy-start(bf16[768,2048]{1,0:T(8,128)(2,1)} %copy-done) | copy-start | bytes 9437188
  468.9 1.2 copy-start.2
  470.1 6.5 %copy-start.13 = (f32[512]{0:T(512)S(1)}, f32[512]{0:T(512)}, u32[]{:S(2)}) copy-start(f32[512]{0:T(512)} %param.29) | copy-start | bytes 6148
Sparse Core Ops, SparseCore 0:
  37.7 22.9 all-gather.2
  318.7 45.3 all-gather.4
